TPU v7x, 128 devices: a whole 4x4x4 slice. The times are simulated.
128 devices in a mesh: sp: 16 (over z, y), tp: 8 (over x, core).
Axes of the slice: x: 4, y: 4, z: 4, core: 2. Of those that a mesh axis runs over, the one named last changes fastest.
Arguments:
- inputs: bfloat16 [16384, 2048], P('sp'), may hold values from -6 to 6
- norm_gain: float32 [3, 2048], replicated, may hold values from 0.1 to 1.9
- query_weight: bfloat16 [3, 2048, 1024], P(None, 'sp', 'tp'), may hold values from -64 to 64
- key_weight: bfloat16 [3, 2048, 512], P(None, 'sp', 'tp'), may hold values from -4 to 4
- value_weight: bfloat16 [3, 2048, 512], P(None, 'sp', 'tp'), may hold values from -0.125 to 0.125
- output_weight: bfloat16 [3, 2048, 1024], P(None, 'sp', 'tp'), may hold values from -0.1875 to 0.1875
- sink_logit: float32 [3, 16], P(None, 'tp'), may hold values from 2 to 7
- final_gain: float32 [2048], replicated, may hold values from 0.1 to 1.9
Outputs:
- result: float32 [16384, 2048], P(('sp', 'tp'))
All inputs are finite; a program needn't handle non-finite values.
Results may differ from a plain program's by a relative error of at most 0.015.
Values may be sent and summed in bfloat16 or wider, within the bound.
A program may use at most 64 MiB of HBM per device.

v0:
```python
import jax
import jax.numpy as jnp
from jax import lax
from jax.sharding import PartitionSpec as P

D = 2048
HEAD_DIM = 64
WINDOW = 128
LAYERS = 3
EPS = 1e-06


def sent_together(arrays, axis, dim, along):
    both = jnp.concatenate(arrays, axis=along)
    result, at, done = (lax.all_gather(both, axis, axis=dim, tiled=True), 0, [])
    for a in arrays:
        done.append(lax.slice_in_dim(result, at, at + a.shape[along], axis=along))
        at += a.shape[along]
    return tuple(done)


def extended_2(block, sides, width):
    for axis, dim in sides:
        count = lax.axis_size(axis)
        forward = [(i, i + 1) for i in range(count - 1)]
        backward = [(target, source) for source, target in forward]
        low = lax.ppermute(
            lax.slice_in_dim(block, block.shape[dim] - width, None, axis=dim), axis, forward
        )
        high = lax.ppermute(lax.slice_in_dim(block, 0, width, axis=dim), axis, backward)
        block = jnp.concatenate([low, block, high], axis=dim)
    return block


def norm_rows(values, gain):
    wide_values = values.astype(jnp.float32)
    inv_root = lax.rsqrt(jnp.mean(wide_values * wide_values, axis=-1, keepdims=True) + EPS)
    return wide_values * inv_root * gain


def rotate(values, places):
    half_dim = values.shape[-1] // 2
    inverse = 10000.0 ** (-jnp.arange(half_dim).astype(jnp.float32) / half_dim)
    angles = places[:, None] * inverse[None, :]
    cosine_table = jnp.cos(angles)[:, None, :]
    sine_table = jnp.sin(angles)[:, None, :]
    front_half = values[..., :half_dim]
    back_half = values[..., half_dim:]
    return jnp.concatenate(
        [
            front_half * cosine_table - back_half * sine_table,
            back_half * cosine_table + front_half * sine_table,
        ],
        axis=-1,
    )


def attend(queries, key_rows, value_rows, sink_row, allowed):
    scores = jnp.einsum(
        "qkgd,skd->kgqs", queries, key_rows, preferred_element_type=jnp.float32
    ) * queries.shape[-1] ** (-0.5)
    scores = jnp.where(allowed[None, None], scores, -jnp.inf)
    sink_col = sink_row[:, :, None]
    largest = jnp.maximum(jnp.max(scores, axis=-1), sink_col)
    powers = jnp.exp(scores - largest[..., None])
    denominator = jnp.sum(powers, axis=-1) + jnp.exp(sink_col - largest)
    weights = (powers / denominator[..., None]).astype(jnp.bfloat16)
    blended = jnp.einsum("kgqs,skd->qkgd", weights, value_rows, preferred_element_type=jnp.float32)
    return blended.astype(jnp.bfloat16)


def shards(
    inputs, norm_gain, query_weight, key_weight, value_weight, output_weight, sink_logit, final_gain
):
    tokens = inputs.shape[0]
    local_heads = query_weight.shape[2] // HEAD_DIM
    local_groups = key_weight.shape[2] // HEAD_DIM
    per_group = local_heads // local_groups
    kv_cols = local_groups * HEAD_DIM
    offset = lax.axis_index("sp") * tokens
    seq_total = tokens * lax.axis_size("sp")
    query_pos = offset + jnp.arange(tokens, dtype=jnp.int32)
    places = query_pos.astype(jnp.float32)
    key_pos = offset - WINDOW + jnp.arange(tokens + 2 * WINDOW, dtype=jnp.int32)
    allowed = (
        (jnp.abs(key_pos[None, :] - query_pos[:, None]) <= WINDOW)
        & (key_pos[None, :] >= 0)
        & (key_pos[None, :] < seq_total)
    )
    whole_query, whole_key, whole_value, whole_out = sent_together(
        (query_weight, key_weight, value_weight, output_weight), "sp", 1, 2
    )
    current = inputs
    final_rows = inputs
    for layer in range(LAYERS):
        normed = norm_rows(current, norm_gain[layer]).astype(jnp.bfloat16)
        query_raw = jnp.dot(normed, whole_query[layer], preferred_element_type=jnp.float32)
        key_raw = jnp.dot(normed, whole_key[layer], preferred_element_type=jnp.float32)
        value_raw = jnp.dot(normed, whole_value[layer], preferred_element_type=jnp.float32)
        out_weight = whole_out[layer]
        queries = rotate(
            (query_raw * float(D) ** (-0.5)).reshape(tokens, local_heads, HEAD_DIM), places
        ).astype(jnp.bfloat16)
        key_rot = rotate(
            (key_raw * float(D) ** (-0.5)).reshape(tokens, local_groups, HEAD_DIM), places
        ).astype(jnp.bfloat16)
        packed = jnp.concatenate(
            [key_rot.reshape(tokens, kv_cols), value_raw.astype(jnp.bfloat16)], axis=1
        )
        extended = extended_2(packed, (("sp", 0),), WINDOW)
        key_rows = extended[:, :kv_cols].reshape(-1, local_groups, HEAD_DIM)
        value_all = extended[:, kv_cols:].reshape(-1, local_groups, HEAD_DIM)
        sink_row = sink_logit[layer].reshape(local_groups, per_group)
        attended = attend(
            queries.reshape(tokens, local_groups, per_group, HEAD_DIM),
            key_rows,
            value_all,
            sink_row,
            allowed,
        )
        attended = attended.reshape(tokens, local_heads * HEAD_DIM)

        def project():
            return lax.dot_general(
                attended, out_weight, (((1,), (1,)), ((), ())), preferred_element_type=jnp.float32
            )

        if layer < LAYERS - 1:
            share_rows = lax.psum_scatter(project(), "tp", scatter_dimension=0, tiled=True).astype(
                jnp.bfloat16
            )
            current = lax.all_gather(share_rows, "tp", axis=0, tiled=True)
        else:
            final_rows = lax.psum_scatter(
                project().astype(jnp.bfloat16), "tp", scatter_dimension=0, tiled=True
            )
    return norm_rows(final_rows, final_gain)


def solution(mesh):
    in_specs = (
        P("sp", None),
        P(),
        P(None, "sp", "tp"),
        P(None, "sp", "tp"),
        P(None, "sp", "tp"),
        P(None, "sp", "tp"),
        P(None, "tp"),
        P(),
    )
    out_specs = P(("sp", "tp"), None)
    return jax.shard_map(shards, mesh=mesh, in_specs=in_specs, out_specs=out_specs, check_vma=False)
```

profile of v0, /device:TPU:0, one launch (start us, length us, event | category | flops | bytes accessed | tf_op | source)
XLA Modules:
  0.0 389.5 jit_solution(7353681811122570966)
XLA Ops:
  6.5 0.9 copy.9
  7.5 0.9 copy.10
  8.4 1.8 pad_maximum_fusion.3
  10.3 1.1 slice_reduce_fusion
  11.4 3.2 fusion.3
  14.7 0.5 multiply_cosine_fusion
  15.2 3.0 fusion.5
  18.2 2.2 fusion.22
  20.4 46.3 %all-gather.4.cloned.1.call-done = bf16[3,2048,384]{2,1,0:T(8,128)(2,1)} async-done(((bf16[3,128,384]{2,1,0:T(8,128)(2,1)}), bf16[3,2048,384]{2,1,0:T(8,128)(2,1)}) %all-gather.4.cloned.1.call-update) | async-done | bytes 4718608 | tf_op jit(solution)/shard_map/all_gather | solution.py:15
  66.8 3.9 fusion.34
  70.6 0.6 fusion.80
  71.2 2.5 convolution_convert_fusion.3
  73.7 3.4 collective-permute-start
  77.1 1.8 collective-permute-start.1
  78.9 2.6 convolution_multiply_fusion.2
  81.5 0.1 subtract_convert_fusion.2
  81.6 1.4 collective-permute-done.1
  83.0 2.2 fusion.12
  85.3 2.5 fusion
  87.8 0.1 exponential_add_fusion.2
  87.9 3.5 fusion.23
  91.4 5.6 %fusion.38 = f32[1024,2048]{1,0:T(8,128)} fusion(bf16[1024,128]{0,1:T(8,128)(2,1)S(1)} %bitcast.174, bf16[3,2048,384]{2,1,0:T(8,128)(2,1)} %all-gather.4.cloned.1.call-done), kind=kOutput, calls=%fused_computation.69 | convolution fusion | flops 536870912 | bytes 9175040 | tf_op jit(solution)/shard_map/dot_general | solution.py:124
  97.0 55.1 %reduce-scatter.4.cloned.1.call-done = f32[128,2048]{1,0:T(8,128)} async-done(((f32[1024,2048]{1,0:T(8,128)}), f32[128,2048]{1,0:T(8,128)}) %reduce-scatter.4.cloned.1.call-update) | async-done | bytes 1048592 | tf_op jit(solution)/shard_map/reduce_scatter | solution.py:129
  152.2 2.1 convert_element_type.126
  154.3 0.2 reduce-scatter.6.cloned.1.call-start
  154.5 31.6 %all-gather.6.cloned.1.call-done = bf16[1024,2048]{1,0:T(8,128)(2,1)} async-done(((bf16[128,2048]{1,0:T(8,128)(2,1)}), bf16[1024,2048]{1,0:T(8,128)(2,1)}) %all-gather.6.cloned.1.call-update) | async-done | bytes 4194320 | tf_op jit(solution)/shard_map/all_gather | solution.py:132
  186.1 3.2 fusion.6
  189.3 0.2 copy-done.3
  189.5 1.0 fusion.8
  190.6 2.5 fusion.33
  193.0 0.6 fusion.78
  193.6 2.5 convolution_convert_fusion.2
  196.1 3.4 collective-permute-start.2
  199.5 1.3 collective-permute-start.3
  200.8 2.6 convolution_multiply_fusion.1
  203.4 0.1 subtract_convert_fusion.1
  203.5 1.8 collective-permute-done.3
  205.4 2.2 fusion.13
  207.7 2.5 fusion.1
  210.2 0.1 exponential_add_fusion.1
  210.3 3.5 fusion.26
  213.8 5.6 %fusion.37 = f32[1024,2048]{1,0:T(8,128)} fusion(bf16[1024,128]{0,1:T(8,128)(2,1)S(1)} %bitcast.175, bf16[3,2048,384]{2,1,0:T(8,128)(2,1)} %all-gather.4.cloned.1.call-done), kind=kOutput, calls=%fused_computation.64 | convolution fusion | flops 536870912 | bytes 9175040 | tf_op jit(solution)/shard_map/dot_general | solution.py:124
  219.4 54.0 %reduce-scatter.6.cloned.1.call-done = f32[128,2048]{1,0:T(8,128)} async-done(((f32[1024,2048]{1,0:T(8,128)}), f32[128,2048]{1,0:T(8,128)}) %reduce-scatter.6.cloned.1.call-update) | async-done | bytes 1048592 | tf_op jit(solution)/shard_map/reduce_scatter | solution.py:129
  273.5 2.1 convert_element_type.134
  275.6 0.3 reduce-scatter.8.cloned.1.call-start
  275.8 31.5 %all-gather.8.cloned.1.call-done = bf16[1024,2048]{1,0:T(8,128)(2,1)} async-done(((bf16[128,2048]{1,0:T(8,128)(2,1)}), bf16[1024,2048]{1,0:T(8,128)(2,1)}) %all-gather.8.cloned.1.call-update) | async-done | bytes 4194320 | tf_op jit(solution)/shard_map/all_gather | solution.py:132
  307.4 3.2 fusion.9
  310.6 0.2 copy-done.2
  310.8 1.0 fusion.11
  311.8 2.4 fusion.32
  314.3 0.6 fusion.76
  314.8 2.5 convolution_convert_fusion.1
  317.4 3.4 collective-permute-start.4
  320.8 1.3 collective-permute-start.5
  322.1 2.6 convolution_multiply_fusion
  324.7 1.8 collective-permute-done.5
  326.6 2.2 fusion.14
  329.0 2.5 fusion.2
  331.4 0.1 exponential_add_fusion
  331.5 3.5 fusion.29
  335.1 4.3 %convolution_convert_fusion = bf16[1024,2048]{1,0:T(8,128)(2,1)} fusion(bf16[1024,128]{0,1:T(8,128)(2,1)S(1)} %bitcast.176, bf16[3,2048,384]{2,1,0:T(8,128)(2,1)} %all-gather.4.cloned.1.call-done), kind=kOutput, calls=%fused_computation.39 | convolution fusion | flops 538968064 | bytes 4980736 | tf_op jit(solution)/shard_map/dot_general | solution.py:124
  339.4 39.6 %reduce-scatter.8.cloned.1.call-done = bf16[128,2048]{1,0:T(8,128)(2,1)} async-done(((bf16[1024,2048]{1,0:T(8,128)(2,1)}), bf16[128,2048]{1,0:T(8,128)(2,1)}) %reduce-scatter.8.cloned.1.call-update) | async-done | bytes 524304 | tf_op jit(solution)/shard_map/reduce_scatter | solution.py:134
  379.0 1.2 fusion.35
  380.2 2.2 fusion.36
  (43 shorter events, 0.8 us)
Async XLA Ops:
  6.5 8.7 %copy-start.4 = (f32[3,2048]{1,0:T(4,128)S(1)}, f32[3,2048]{1,0:T(4,128)}, u32[]{:S(2)}) copy-start(f32[3,2048]{1,0:T(4,128)} %param.9) | copy-start | bytes 73732
  6.5 60.2 %all-gather.4.cloned.1.call-start = ((), (), s32[]{:S(2)}) async-start(), calls=%async_computation.3 | async-start | bytes 5013504 | tf_op jit(solution)/shard_map/all_gather | solution.py:15
  10.2 142.0 %reduce-scatter.4.cloned.1.call-start = ((), (), s32[]{:S(2)}) async-start(), calls=%async_computation.4 | async-start | bytes 9437184 | tf_op jit(solution)/shard_map/reduce_scatter | solution.py:129
  10.3 5.0 %copy-start.1 = (bf16[1024,2048]{1,0:T(8,128)(2,1)S(1)}, bf16[1024,2048]{1,0:T(8,128)(2,1)}, u32[]{:S(2)}) copy-start(bf16[1024,2048]{1,0:T(8,128)(2,1)} %param.8) | copy-start | bytes 12582916
  66.8 4.4 %copy-start = (bf16[1024,2048]{1,0:T(8,128)(2,1)S(1)}, bf16[1024,2048]{1,0:T(8,128)(2,1)}, u32[]{:S(2)}) copy-start(bf16[1024,2048]{1,0:T(8,128)(2,1)} %fusion.5) | copy-start | bytes 12582916
  73.7 7.8 %collective-permute-start = (bf16[128,128]{0,1:T(8,128)(2,1)S(1)}, bf16[128,128]{0,1:T(8,128)(2,1)S(1)}, u32[]{:S(2)}, u32[]{:S(2)}) collective-permute-start(bf16[128,128]{0,1:T(8,128)(2,1)S(1)} %get-tuple-element.24), channel_id=1, source_target_pairs={{0,8},{8,16},{16,24},{24,32},{32,40},{40,48},{48,56},{56,64},{64,7... | collective-permute-start | bytes 98312 | tf_op jit(solution)/shard_map/ppermute | solution.py:27
  77.1 5.8 %collective-permute-start.1 = (bf16[128,128]{0,1:T(8,128)(2,1)S(1)}, bf16[128,128]{0,1:T(8,128)(2,1)S(1)}, u32[]{:S(2)}, u32[]{:S(2)}) collective-permute-start(bf16[128,128]{0,1:T(8,128)(2,1)S(1)} %get-tuple-element.25), channel_id=1, source_target_pairs={{8,0},{16,8},{24,16},{32,24},{40,32},{48,40},{56,48},{64,56},{72,6... | collective-permute-start | bytes 98312 | tf_op jit(solution)/shard_map/ppermute | solution.py:30
  97.0 89.1 %all-gather.6.cloned.1.call-start = ((), (), s32[]{:S(2)}) async-start(), calls=%async_computation.5 | async-start | bytes 4718592 | tf_op jit(solution)/shard_map/all_gather | solution.py:132
  154.3 119.2 %reduce-scatter.6.cloned.1.call-start = ((), (), s32[]{:S(2)}) async-start(), calls=%async_computation.6 | async-start | bytes 9437184 | tf_op jit(solution)/shard_map/reduce_scatter | solution.py:129
  186.1 3.4 copy-start.3
  196.1 7.4 %collective-permute-start.2 = (bf16[128,128]{0,1:T(8,128)(2,1)S(1)}, bf16[128,128]{0,1:T(8,128)(2,1)S(1)}, u32[]{:S(2)}, u32[]{:S(2)}) collective-permute-start(bf16[128,128]{0,1:T(8,128)(2,1)S(1)} %get-tuple-element.22), channel_id=1, source_target_pairs={{0,8},{8,16},{16,24},{24,32},{32,40},{40,48},{48,56},{56,64},{64,7... | collective-permute-start | bytes 98312 | tf_op jit(solution)/shard_map/ppermute | solution.py:27
  199.5 5.8 %collective-permute-start.3 = (bf16[128,128]{0,1:T(8,128)(2,1)S(1)}, bf16[128,128]{0,1:T(8,128)(2,1)S(1)}, u32[]{:S(2)}, u32[]{:S(2)}) collective-permute-start(bf16[128,128]{0,1:T(8,128)(2,1)S(1)} %get-tuple-element.23), channel_id=1, source_target_pairs={{8,0},{16,8},{24,16},{32,24},{40,32},{48,40},{56,48},{64,56},{72,6... | collective-permute-start | bytes 98312 | tf_op jit(solution)/shard_map/ppermute | solution.py:30
  219.4 88.0 %all-gather.8.cloned.1.call-start = ((), (), s32[]{:S(2)}) async-start(), calls=%async_computation.7 | async-start | bytes 4718592 | tf_op jit(solution)/shard_map/all_gather | solution.py:132
  275.6 103.4 %reduce-scatter.8.cloned.1.call-start = ((), (), s32[]{:S(2)}) async-start(), calls=%async_computation.8 | async-start | bytes 4718592 | tf_op jit(solution)/shard_map/reduce_scatter | solution.py:134
  307.4 3.4 copy-start.2
  317.4 7.4 %collective-permute-start.4 = (bf16[128,128]{0,1:T(8,128)(2,1)S(1)}, bf16[128,128]{0,1:T(8,128)(2,1)S(1)}, u32[]{:S(2)}, u32[]{:S(2)}) collective-permute-start(bf16[128,128]{0,1:T(8,128)(2,1)S(1)} %get-tuple-element.20), channel_id=1, source_target_pairs={{0,8},{8,16},{16,24},{24,32},{32,40},{40,48},{48,56},{56,64},{64,7... | collective-permute-start | bytes 98312 | tf_op jit(solution)/shard_map/ppermute | solution.py:27
  320.8 5.8 %collective-permute-start.5 = (bf16[128,128]{0,1:T(8,128)(2,1)S(1)}, bf16[128,128]{0,1:T(8,128)(2,1)S(1)}, u32[]{:S(2)}, u32[]{:S(2)}) collective-permute-start(bf16[128,128]{0,1:T(8,128)(2,1)S(1)} %get-tuple-element.21), channel_id=1, source_target_pairs={{8,0},{16,8},{24,16},{32,24},{40,32},{48,40},{56,48},{64,56},{72,6... | collective-permute-start | bytes 98312 | tf_op jit(solution)/shard_map/ppermute | solution.py:30
  335.1 45.1 %copy-start.5 = (f32[2048]{0:T(1024)S(1)}, f32[2048]{0:T(1024)}, u32[]{:S(2)}) copy-start(f32[2048]{0:T(1024)} %param.15) | copy-start | bytes 24580
Sparse Core Ops, SparseCore 0:
  10.3 56.4 all-gather.3
  97.1 55.0 reduce-scatter.3
  154.4 31.6 all-gather.5
  219.5 53.9 reduce-scatter.5
  275.7 31.6 all-gather.7
  339.5 39.4 reduce-scatter.7
where the time goes:
time: 395 us; the launch traced here: 389 us
  waiting for transfers between devices  263 us (67%)
  matrix products  56.7 us (14%)
  other arithmetic  36.8 us (9%)
  starting transfers between devices  15.1 us (4%)
  between operations  14.1 us (4%)
    reduce_scatter x2, waiting for transfers between devices, shards(): lax.psum_scatter(project(), 'tp', scatter_dimension=0, tiled=True)  109 us
    all_gather x2, waiting for transfers between devices, shards(): current = lax.all_gather(share_rows, 'tp', axis=0, tiled=True)  63.1 us
    all_gather x1, waiting for transfers between devices, sent_together(): result, at, done = (lax.all_gather(both, axis, axis=dim, tiled=True), 0, [])  46.3 us
    reduce_scatter x1, waiting for transfers between devices, shards(): lax.psum_scatter(project().astype(jnp.bfloat16), 'tp', scatter_dimension=...  39.6 us
    dot_general x3, matrix products, project(): lax.dot_general(attended, out_weight, (((1,), (1,)), ((), ())), preferred...  15.4 us
    reduce_sum x4, other arithmetic, norm_rows(): jnp.mean(wide_values * wide_values, axis=-1, keepdims=True) + EPS  10.9 us
    dot_general x3, matrix products, attend(): jnp.einsum('kgqs,skd->qkgd', weights, value_rows, preferred_element_type=...  10.6 us
    ppermute x3, starting transfers between devices, extended_2(): lax.ppermute(lax.slice_in_dim(block, block.shape[dim] - width, None, axis...  10.2 us
  transfers between devices with their start and end apart: 12, of which 9 were waited for; matrix products, arithmetic and copies ran while one was open for 5% of the time, Pallas kernels for 0%

commit v1 on v0

--- a/solution.py
+++ b/solution.py
@@ -129,7 +129,36 @@
             share_rows = lax.psum_scatter(project(), "tp", scatter_dimension=0, tiled=True).astype(
                 jnp.bfloat16
             )
-            current = lax.all_gather(share_rows, "tp", axis=0, tiled=True)
+
+            def process_counts_on_mesh(m):
+                axis_name = "tp"
+                last = lax.axis_size(axis_name)
+                formed = lax.axis_index(axis_name)
+                piece_out, shaped, known = (last, formed, m.shape[0])
+                windows = tuple((k * piece_out if w == 0 else k for w, k in enumerate(m.shape)))
+                near = jnp.zeros(windows, m.dtype)
+                placed = lax.dynamic_update_slice_in_dim(near, m, shaped * known, axis=0)
+                reply = u1 = m
+                num = 1
+                while num < piece_out // 2 + 1:
+                    e_next = tuple(((w, (w + 1) % piece_out) for w in range(piece_out)))
+                    reply = lax.ppermute(reply, axis_name=axis_name, perm=e_next)
+                    placed = lax.dynamic_update_slice_in_dim(
+                        placed, reply, (shaped - num) % piece_out * known, axis=0
+                    )
+                    if 2 * num < piece_out:
+                        u1 = lax.ppermute(
+                            u1,
+                            axis_name=axis_name,
+                            perm=tuple(((w, (w - 1) % piece_out) for w in range(piece_out))),
+                        )
+                        placed = lax.dynamic_update_slice_in_dim(
+                            placed, u1, (shaped + num) % piece_out * known, axis=0
+                        )
+                    num += 1
+                return placed
+
+            current = process_counts_on_mesh(share_rows)
         else:
             final_rows = lax.psum_scatter(
                 project().astype(jnp.bfloat16), "tp", scatter_dimension=0, tiled=True

time: 395 us -> 408 us (1.033)
  starting transfers between devices: 15.1 us -> 34.6 us
  waiting for transfers between devices: 263 us -> 250 us
  local copies, waits for them, and re-layouts: 3.38 us -> 13.9 us
    all_gather x2 -> x0, waiting for transfers between devices: 63.1 us -> none  [shards(): current = lax.all_gather(share_rows, 'tp', axis=0, tiled=True)]
    ppermute x0 -> x14, waiting for transfers between devices: none -> 54.3 us  [the longest x8 53.4 us: process_counts_on_mesh(): reply = lax.ppermute(reply, axis_name=axis_name, perm=e_next)]
    ppermute x0 -> x14, starting transfers between devices: none -> 17.9 us  [the longest x6 17.8 us: process_counts_on_mesh(): lax.ppermute(u1, axis_name=axis_name, perm=tuple(((w, (w - 1) % piece_out...]
    dynamic_update_slice x0 -> x14, local copies, waits for them, and re-layouts: none -> 7.23 us  [the longest x6 3.7 us: process_counts_on_mesh(): lax.dynamic_update_slice_in_dim(placed, u1, (shaped + num) % piece_out *...]
    convert_element_type x2 -> x0, other arithmetic: 4.17 us -> none  [shards(): lax.psum_scatter(project(), 'tp', scatter_dimension=0, tiled=True)]
  transfers between devices with their start and end apart: 12 -> 24, of which waited for: 9 -> 15; matrix products, arithmetic and copies ran while one was open for 5% -> 6% of each run, Pallas kernels for 0% -> 0%
where the time goes in v1:
time: 408 us; the launch traced here: 402 us
  waiting for transfers between devices  250 us (61%)
  matrix products  56.7 us (14%)
  starting transfers between devices  34.6 us (8%)
  other arithmetic  33.4 us (8%)
  local copies, waits for them, and re-layouts  13.9 us (3%)
  between operations  13.9 us (3%)
    reduce_scatter x2, waiting for transfers between devices, shards(): lax.psum_scatter(project(), 'tp', scatter_dimension=0, tiled=True)  108 us
    ppermute x8, waiting for transfers between devices, process_counts_on_mesh(): reply = lax.ppermute(reply, axis_name=axis_name, perm=e_next)  53.4 us
    all_gather x1, waiting for transfers between devices, sent_together(): result, at, done = (lax.all_gather(both, axis, axis=dim, tiled=True), 0, [])  46.3 us
    reduce_scatter x1, waiting for transfers between devices, shards(): lax.psum_scatter(project().astype(jnp.bfloat16), 'tp', scatter_dimension=...  38.5 us
    ppermute x6, starting transfers between devices, process_counts_on_mesh(): lax.ppermute(u1, axis_name=axis_name, perm=tuple(((w, (w - 1) % piece_out...  17.8 us
    dot_general x3, matrix products, project(): lax.dot_general(attended, out_weight, (((1,), (1,)), ((), ())), preferred...  15.4 us
    ppermute x3, starting transfers between devices, extended_2(): lax.ppermute(lax.slice_in_dim(block, block.shape[dim] - width, None, axis...  11.5 us
    dot_general x3, matrix products, attend(): jnp.einsum('kgqs,skd->qkgd', weights, value_rows, preferred_element_type=...  10.6 us
  transfers between devices with their start and end apart: 24, of which 15 were waited for; matrix products, arithmetic and copies ran while one was open for 6% of the time, Pallas kernels for 0%

profile of v1, /device:TPU:0, one launch (start us, length us, event | category | flops | bytes accessed | tf_op | source)
XLA Modules:
  0.0 402.4 jit_solution(4769108914522220408)
XLA Ops:
  6.5 0.9 copy.10
  7.5 0.9 copy.9
  8.4 1.8 pad_maximum_fusion.3
  10.3 1.1 slice_reduce_fusion
  11.4 3.2 fusion.3
  15.2 3.0 fusion.5
  18.2 2.2 fusion.22
  20.4 46.3 %all-gather.2.cloned.1.call-done = bf16[3,2048,384]{2,1,0:T(8,128)(2,1)} async-done(((bf16[3,128,384]{2,1,0:T(8,128)(2,1)}), bf16[3,2048,384]{2,1,0:T(8,128)(2,1)}) %all-gather.2.cloned.1.call-update) | async-done | bytes 4718608 | tf_op jit(solution)/shard_map/all_gather | solution.py:15
  66.8 3.9 fusion.34
  71.2 2.5 convolution_convert_fusion.3
  73.7 3.4 collective-permute-start
  77.1 1.6 collective-permute-start.1
  78.7 2.6 convolution_multiply_fusion.2
  81.4 1.6 collective-permute-done.1
  83.0 2.2 fusion.12
  85.3 2.5 fusion
  87.9 3.5 fusion.23
  91.4 5.6 %fusion.38 = f32[1024,2048]{1,0:T(8,128)} fusion(bf16[1024,128]{0,1:T(8,128)(2,1)S(1)} %bitcast.174, bf16[3,2048,384]{2,1,0:T(8,128)(2,1)} %all-gather.2.cloned.1.call-done), kind=kOutput, calls=%fused_computation.69 | convolution fusion | flops 536870912 | bytes 9175040 | tf_op jit(solution)/shard_map/dot_general | solution.py:124
  97.6 54.6 %reduce-scatter.4.cloned.1.call-done = f32[128,2048]{1,0:T(8,128)} async-done(((f32[1024,2048]{1,0:T(8,128)}), f32[128,2048]{1,0:T(8,128)}) %reduce-scatter.4.cloned.1.call-update) | async-done | bytes 1048592 | tf_op jit(solution)/shard_map/reduce_scatter | solution.py:129
  152.2 2.5 broadcast.326.clone
  154.7 0.9 constant_dynamic-update-slice_fusion.15
  155.6 3.0 collective-permute-start.3
  158.5 6.9 %collective-permute-done.2 = bf16[128,2048]{1,0:T(8,128)(2,1)S(1)} collective-permute-done((bf16[128,2048]{1,0:T(8,128)(2,1)S(1)}, bf16[128,2048]{1,0:T(8,128)(2,1)S(1)}, u32[]{:S(2)}, u32[]{:S(2)}) %collective-permute-start.2) | collective-permute-done | bytes 524320 | tf_op jit(solution)/shard_map/ppermute | solution.py:145
  165.4 3.1 collective-permute-start.5
  168.5 6.8 %collective-permute-done.4 = bf16[128,2048]{1,0:T(8,128)(2,1)S(1)} collective-permute-done((bf16[128,2048]{1,0:T(8,128)(2,1)S(1)}, bf16[128,2048]{1,0:T(8,128)(2,1)S(1)}, u32[]{:S(2)}, u32[]{:S(2)}) %collective-permute-start.4) | collective-permute-done | bytes 524320 | tf_op jit(solution)/shard_map/ppermute | solution.py:145
  176.0 1.9 constant_dynamic-update-slice_fusion.13
  177.9 3.0 collective-permute-start.7
  181.7 3.3 collective-permute-done.6
  186.7 0.9 collective-permute-done.7
  188.4 6.4 %collective-permute-done.8 = bf16[128,2048]{1,0:T(8,128)(2,1)S(1)} collective-permute-done((bf16[128,2048]{1,0:T(8,128)(2,1)S(1)}, bf16[128,2048]{1,0:T(8,128)(2,1)S(1)}, u32[]{:S(2)}, u32[]{:S(2)}) %collective-permute-start.8) | collective-permute-done | bytes 524320 | tf_op jit(solution)/shard_map/ppermute | solution.py:145
  195.7 3.1 fusion.6
  198.8 3.2 fusion.8
  202.0 2.5 fusion.33
  205.0 2.5 convolution_convert_fusion.2
  207.6 1.3 collective-permute-start.10
  208.9 4.7 %collective-permute-start.9 = (bf16[128,128]{0,1:T(8,128)(2,1)S(1)}, bf16[128,128]{0,1:T(8,128)(2,1)S(1)}, u32[]{:S(2)}, u32[]{:S(2)}) collective-permute-start(bf16[128,128]{0,1:T(8,128)(2,1)S(1)} %get-tuple-element.26), channel_id=1, source_target_pairs={{0,8},{8,16},{16,24},{24,32},{32,40},{40,48},{48,56},{56,64},{64,7... | collective-permute-start | bytes 98312 | tf_op jit(solution)/shard_map/ppermute | solution.py:27
  213.6 2.6 convolution_multiply_fusion.1
  216.3 2.2 fusion.13
  218.6 2.5 fusion.1
  221.2 3.5 fusion.26
  224.7 5.6 %fusion.37 = f32[1024,2048]{1,0:T(8,128)} fusion(bf16[1024,128]{0,1:T(8,128)(2,1)S(1)} %bitcast.175, bf16[3,2048,384]{2,1,0:T(8,128)(2,1)} %all-gather.2.cloned.1.call-done), kind=kOutput, calls=%fused_computation.64 | convolution fusion | flops 536870912 | bytes 9175040 | tf_op jit(solution)/shard_map/dot_general | solution.py:124
  230.6 53.0 %reduce-scatter.6.cloned.1.call-done = f32[128,2048]{1,0:T(8,128)} async-done(((f32[1024,2048]{1,0:T(8,128)}), f32[128,2048]{1,0:T(8,128)}) %reduce-scatter.6.cloned.1.call-update) | async-done | bytes 1048592 | tf_op jit(solution)/shard_map/reduce_scatter | solution.py:129
  284.9 2.9 collective-permute-start.12
  287.9 6.9 %collective-permute-done.11 = bf16[128,2048]{1,0:T(8,128)(2,1)S(1)} collective-permute-done((bf16[128,2048]{1,0:T(8,128)(2,1)S(1)}, bf16[128,2048]{1,0:T(8,128)(2,1)S(1)}, u32[]{:S(2)}, u32[]{:S(2)}) %collective-permute-start.11) | collective-permute-done | bytes 524320 | tf_op jit(solution)/shard_map/ppermute | solution.py:145
  294.7 3.0 collective-permute-start.14
  297.7 6.9 %collective-permute-done.13 = bf16[128,2048]{1,0:T(8,128)(2,1)S(1)} collective-permute-done((bf16[128,2048]{1,0:T(8,128)(2,1)S(1)}, bf16[128,2048]{1,0:T(8,128)(2,1)S(1)}, u32[]{:S(2)}, u32[]{:S(2)}) %collective-permute-start.13) | collective-permute-done | bytes 524320 | tf_op jit(solution)/shard_map/ppermute | solution.py:145
  304.7 3.0 collective-permute-start.16
  307.7 6.7 %collective-permute-done.15 = bf16[128,2048]{1,0:T(8,128)(2,1)S(1)} collective-permute-done((bf16[128,2048]{1,0:T(8,128)(2,1)S(1)}, bf16[128,2048]{1,0:T(8,128)(2,1)S(1)}, u32[]{:S(2)}, u32[]{:S(2)}) %collective-permute-start.15) | collective-permute-done | bytes 524320 | tf_op jit(solution)/shard_map/ppermute | solution.py:145
  314.6 9.6 %collective-permute-done.17 = bf16[128,2048]{1,0:T(8,128)(2,1)S(1)} collective-permute-done((bf16[128,2048]{1,0:T(8,128)(2,1)S(1)}, bf16[128,2048]{1,0:T(8,128)(2,1)S(1)}, u32[]{:S(2)}, u32[]{:S(2)}) %collective-permute-start.17) | collective-permute-done | bytes 524320 | tf_op jit(solution)/shard_map/ppermute | solution.py:145
  324.2 0.9 fusion.9
  325.1 1.0 fusion.11
  326.2 2.4 fusion.32
  329.2 2.5 convolution_convert_fusion.1
  331.7 3.4 collective-permute-start.18
  335.1 1.5 collective-permute-start.19
  336.7 2.6 convolution_multiply_fusion
  339.3 1.6 collective-permute-done.19
  341.0 2.2 fusion.14
  343.3 2.5 fusion.2
  345.9 3.5 fusion.29
  349.4 4.3 %convolution_convert_fusion = bf16[1024,2048]{1,0:T(8,128)(2,1)} fusion(bf16[1024,128]{0,1:T(8,128)(2,1)S(1)} %bitcast.176, bf16[3,2048,384]{2,1,0:T(8,128)(2,1)} %all-gather.2.cloned.1.call-done), kind=kOutput, calls=%fused_computation.39 | convolution fusion | flops 538968064 | bytes 4980736 | tf_op jit(solution)/shard_map/dot_general | solution.py:124
  353.7 38.5 %reduce-scatter.8.cloned.1.call-done = bf16[128,2048]{1,0:T(8,128)(2,1)} async-done(((bf16[1024,2048]{1,0:T(8,128)(2,1)}), bf16[128,2048]{1,0:T(8,128)(2,1)}) %reduce-scatter.8.cloned.1.call-update) | async-done | bytes 524304 | tf_op jit(solution)/shard_map/reduce_scatter | solution.py:163
  392.2 1.2 fusion.35
  393.4 2.2 fusion.36
  (81 shorter events, 10.8 us)
Async XLA Ops:
  6.5 8.7 %copy-start.4 = (f32[3,2048]{1,0:T(4,128)S(1)}, f32[3,2048]{1,0:T(4,128)}, u32[]{:S(2)}) copy-start(f32[3,2048]{1,0:T(4,128)} %param.9) | copy-start | bytes 73732
  6.5 60.2 %all-gather.2.cloned.1.call-start = ((), (), s32[]{:S(2)}) async-start(), calls=%async_computation.3 | async-start | bytes 5013504 | tf_op jit(solution)/shard_map/all_gather | solution.py:15
  10.2 142.0 %reduce-scatter.4.cloned.1.call-start = ((), (), s32[]{:S(2)}) async-start(), calls=%async_computation.4 | async-start | bytes 9437184 | tf_op jit(solution)/shard_map/reduce_scatter | solution.py:129
  10.3 5.0 %copy-start.1 = (bf16[1024,2048]{1,0:T(8,128)(2,1)S(1)}, bf16[1024,2048]{1,0:T(8,128)(2,1)}, u32[]{:S(2)}) copy-start(bf16[1024,2048]{1,0:T(8,128)(2,1)} %param.8) | copy-start | bytes 12582916
  66.8 4.4 %copy-start = (bf16[1024,2048]{1,0:T(8,128)(2,1)S(1)}, bf16[1024,2048]{1,0:T(8,128)(2,1)}, u32[]{:S(2)}) copy-start(bf16[1024,2048]{1,0:T(8,128)(2,1)} %fusion.5) | copy-start | bytes 12582916
  73.7 7.6 %collective-permute-start = (bf16[128,128]{0,1:T(8,128)(2,1)S(1)}, bf16[128,128]{0,1:T(8,128)(2,1)S(1)}, u32[]{:S(2)}, u32[]{:S(2)}) collective-permute-start(bf16[128,128]{0,1:T(8,128)(2,1)S(1)} %get-tuple-element.28), channel_id=1, source_target_pairs={{0,8},{8,16},{16,24},{24,32},{32,40},{40,48},{48,56},{56,64},{64,7... | collective-permute-start | bytes 98312 | tf_op jit(solution)/shard_map/ppermute | solution.py:27
  77.1 5.8 %collective-permute-start.1 = (bf16[128,128]{0,1:T(8,128)(2,1)S(1)}, bf16[128,128]{0,1:T(8,128)(2,1)S(1)}, u32[]{:S(2)}, u32[]{:S(2)}) collective-permute-start(bf16[128,128]{0,1:T(8,128)(2,1)S(1)} %get-tuple-element.29), channel_id=1, source_target_pairs={{8,0},{16,8},{24,16},{32,24},{40,32},{48,40},{56,48},{64,56},{72,6... | collective-permute-start | bytes 98312 | tf_op jit(solution)/shard_map/ppermute | solution.py:30
  97.0 186.6 %reduce-scatter.6.cloned.1.call-start = ((), (), s32[]{:S(2)}) async-start(), calls=%async_computation.5 | async-start | bytes 9437184 | tf_op jit(solution)/shard_map/reduce_scatter | solution.py:129
  152.2 2.5 copy-start.2
  155.6 9.8 %collective-permute-start.2 = (bf16[128,2048]{1,0:T(8,128)(2,1)S(1)}, bf16[128,2048]{1,0:T(8,128)(2,1)S(1)}, u32[]{:S(2)}, u32[]{:S(2)}) collective-permute-start(bf16[128,2048]{1,0:T(8,128)(2,1)S(1)} %get-tuple-element.11), channel_id=1, source_target_pairs={{0,1},{1,2},{2,3},{3,4},{4,5},{5,6},{6,7},{7,0},{8,9},{9,10},{10,1... | collective-permute-start | bytes 1572872 | tf_op jit(solution)/shard_map/ppermute | solution.py:145
  155.6 9.8 %collective-permute-start.3 = (bf16[128,2048]{1,0:T(8,128)(2,1)S(1)}, bf16[128,2048]{1,0:T(8,128)(2,1)}, u32[]{:S(2)}, u32[]{:S(2)}) collective-permute-start(bf16[128,2048]{1,0:T(8,128)(2,1)S(1)} %get-tuple-element.11), channel_id=1, source_target_pairs={{0,7},{1,0},{2,1},{3,2},{4,3},{5,4},{6,5},{7,6},{8,15},{9,8},{10,9... | collective-permute-start | bytes 1572872 | tf_op jit(solution)/shard_map/ppermute | solution.py:150
  165.4 9.8 %collective-permute-start.4 = (bf16[128,2048]{1,0:T(8,128)(2,1)S(1)}, bf16[128,2048]{1,0:T(8,128)(2,1)S(1)}, u32[]{:S(2)}, u32[]{:S(2)}) collective-permute-start(bf16[128,2048]{1,0:T(8,128)(2,1)S(1)} %collective-permute-done.2), channel_id=1, source_target_pairs={{0,1},{1,2},{2,3},{3,4},{4,5},{5,6},{6,7},{7,0},{8,9},{9,10},{10,1... | collective-permute-start | bytes 1572872 | tf_op jit(solution)/shard_map/ppermute | solution.py:145
  165.4 12.5 %collective-permute-start.5 = (bf16[128,2048]{1,0:T(8,128)(2,1)}, bf16[128,2048]{1,0:T(8,128)(2,1)S(1)}, u32[]{:S(2)}, u32[]{:S(2)}) collective-permute-start(bf16[128,2048]{1,0:T(8,128)(2,1)} %collective-permute-done.3), channel_id=1, source_target_pairs={{0,7},{1,0},{2,1},{3,2},{4,3},{5,4},{6,5},{7,6},{8,15},{9,8},{10,9... | collective-permute-start | bytes 1572872 | tf_op jit(solution)/shard_map/ppermute | solution.py:150
  175.2 9.8 %collective-permute-start.6 = (bf16[128,2048]{1,0:T(8,128)(2,1)S(1)}, bf16[128,2048]{1,0:T(8,128)(2,1)S(1)}, u32[]{:S(2)}, u32[]{:S(2)}) collective-permute-start(bf16[128,2048]{1,0:T(8,128)(2,1)S(1)} %collective-permute-done.4), channel_id=1, source_target_pairs={{0,1},{1,2},{2,3},{3,4},{4,5},{5,6},{6,7},{7,0},{8,9},{9,10},{10,1... | collective-permute-start | bytes 1572872 | tf_op jit(solution)/shard_map/ppermute | solution.py:145
  177.9 9.7 %collective-permute-start.7 = (bf16[128,2048]{1,0:T(8,128)(2,1)S(1)}, bf16[128,2048]{1,0:T(8,128)(2,1)S(1)}, u32[]{:S(2)}, u32[]{:S(2)}) collective-permute-start(bf16[128,2048]{1,0:T(8,128)(2,1)S(1)} %collective-permute-done.5), channel_id=1, source_target_pairs={{0,7},{1,0},{2,1},{3,2},{4,3},{5,4},{6,5},{7,6},{8,15},{9,8},{10,9... | collective-permute-start | bytes 1572872 | tf_op jit(solution)/shard_map/ppermute | solution.py:150
  185.0 9.8 %collective-permute-start.8 = (bf16[128,2048]{1,0:T(8,128)(2,1)S(1)}, bf16[128,2048]{1,0:T(8,128)(2,1)S(1)}, u32[]{:S(2)}, u32[]{:S(2)}) collective-permute-start(bf16[128,2048]{1,0:T(8,128)(2,1)S(1)} %collective-permute-done.6), channel_id=1, source_target_pairs={{0,1},{1,2},{2,3},{3,4},{4,5},{5,6},{6,7},{7,0},{8,9},{9,10},{10,1... | collective-permute-start | bytes 1572872 | tf_op jit(solution)/shard_map/ppermute | solution.py:145
  207.6 8.7 %collective-permute-start.10 = (bf16[128,128]{0,1:T(8,128)(2,1)S(1)}, bf16[128,128]{0,1:T(8,128)(2,1)S(1)}, u32[]{:S(2)}, u32[]{:S(2)}) collective-permute-start(bf16[128,128]{0,1:T(8,128)(2,1)S(1)} %get-tuple-element.27), channel_id=1, source_target_pairs={{8,0},{16,8},{24,16},{32,24},{40,32},{48,40},{56,48},{64,56},{72,6... | collective-permute-start | bytes 98312 | tf_op jit(solution)/shard_map/ppermute | solution.py:30
  208.9 7.4 %collective-permute-start.9 = (bf16[128,128]{0,1:T(8,128)(2,1)S(1)}, bf16[128,128]{0,1:T(8,128)(2,1)S(1)}, u32[]{:S(2)}, u32[]{:S(2)}) collective-permute-start(bf16[128,128]{0,1:T(8,128)(2,1)S(1)} %get-tuple-element.26), channel_id=1, source_target_pairs={{0,8},{8,16},{16,24},{24,32},{32,40},{40,48},{48,56},{56,64},{64,7... | collective-permute-start | bytes 98312 | tf_op jit(solution)/shard_map/ppermute | solution.py:27
  230.3 161.9 %reduce-scatter.8.cloned.1.call-start = ((), (), s32[]{:S(2)}) async-start(), calls=%async_computation.6 | async-start | bytes 4718592 | tf_op jit(solution)/shard_map/reduce_scatter | solution.py:163
  283.6 1.2 copy-start.3
  284.9 9.8 %collective-permute-start.11 = (bf16[128,2048]{1,0:T(8,128)(2,1)S(1)}, bf16[128,2048]{1,0:T(8,128)(2,1)S(1)}, u32[]{:S(2)}, u32[]{:S(2)}) collective-permute-start(bf16[128,2048]{1,0:T(8,128)(2,1)S(1)} %get-tuple-element.9), channel_id=1, source_target_pairs={{0,1},{1,2},{2,3},{3,4},{4,5},{5,6},{6,7},{7,0},{8,9},{9,10},{10,1... | collective-permute-start | bytes 1572872 | tf_op jit(solution)/shard_map/ppermute | solution.py:145
  284.9 9.8 %collective-permute-start.12 = (bf16[128,2048]{1,0:T(8,128)(2,1)S(1)}, bf16[128,2048]{1,0:T(8,128)(2,1)S(1)}, u32[]{:S(2)}, u32[]{:S(2)}) collective-permute-start(bf16[128,2048]{1,0:T(8,128)(2,1)S(1)} %get-tuple-element.9), channel_id=1, source_target_pairs={{0,7},{1,0},{2,1},{3,2},{4,3},{5,4},{6,5},{7,6},{8,15},{9,8},{10,9... | collective-permute-start | bytes 1572872 | tf_op jit(solution)/shard_map/ppermute | solution.py:150
  294.7 9.8 %collective-permute-start.13 = (bf16[128,2048]{1,0:T(8,128)(2,1)S(1)}, bf16[128,2048]{1,0:T(8,128)(2,1)S(1)}, u32[]{:S(2)}, u32[]{:S(2)}) collective-permute-start(bf16[128,2048]{1,0:T(8,128)(2,1)S(1)} %collective-permute-done.11), channel_id=1, source_target_pairs={{0,1},{1,2},{2,3},{3,4},{4,5},{5,6},{6,7},{7,0},{8,9},{9,10},{10,1... | collective-permute-start | bytes 1572872 | tf_op jit(solution)/shard_map/ppermute | solution.py:145
  294.7 9.9 %collective-permute-start.14 = (bf16[128,2048]{1,0:T(8,128)(2,1)S(1)}, bf16[128,2048]{1,0:T(8,128)(2,1)S(1)}, u32[]{:S(2)}, u32[]{:S(2)}) collective-permute-start(bf16[128,2048]{1,0:T(8,128)(2,1)S(1)} %collective-permute-done.12), channel_id=1, source_target_pairs={{0,7},{1,0},{2,1},{3,2},{4,3},{5,4},{6,5},{7,6},{8,15},{9,8},{10,9... | collective-permute-start | bytes 1572872 | tf_op jit(solution)/shard_map/ppermute | solution.py:150
  304.6 9.8 %collective-permute-start.15 = (bf16[128,2048]{1,0:T(8,128)(2,1)S(1)}, bf16[128,2048]{1,0:T(8,128)(2,1)S(1)}, u32[]{:S(2)}, u32[]{:S(2)}) collective-permute-start(bf16[128,2048]{1,0:T(8,128)(2,1)S(1)} %collective-permute-done.13), channel_id=1, source_target_pairs={{0,1},{1,2},{2,3},{3,4},{4,5},{5,6},{6,7},{7,0},{8,9},{9,10},{10,1... | collective-permute-start | bytes 1572872 | tf_op jit(solution)/shard_map/ppermute | solution.py:145
  304.7 9.8 %collective-permute-start.16 = (bf16[128,2048]{1,0:T(8,128)(2,1)S(1)}, bf16[128,2048]{1,0:T(8,128)(2,1)S(1)}, u32[]{:S(2)}, u32[]{:S(2)}) collective-permute-start(bf16[128,2048]{1,0:T(8,128)(2,1)S(1)} %collective-permute-done.14), channel_id=1, source_target_pairs={{0,7},{1,0},{2,1},{3,2},{4,3},{5,4},{6,5},{7,6},{8,15},{9,8},{10,9... | collective-permute-start | bytes 1572872 | tf_op jit(solution)/shard_map/ppermute | solution.py:150
  314.4 9.8 %collective-permute-start.17 = (bf16[128,2048]{1,0:T(8,128)(2,1)S(1)}, bf16[128,2048]{1,0:T(8,128)(2,1)S(1)}, u32[]{:S(2)}, u32[]{:S(2)}) collective-permute-start(bf16[128,2048]{1,0:T(8,128)(2,1)S(1)} %collective-permute-done.15), channel_id=1, source_target_pairs={{0,1},{1,2},{2,3},{3,4},{4,5},{5,6},{6,7},{7,0},{8,9},{9,10},{10,1... | collective-permute-start | bytes 1572872 | tf_op jit(solution)/shard_map/ppermute | solution.py:145
  331.7 7.6 %collective-permute-start.18 = (bf16[128,128]{0,1:T(8,128)(2,1)S(1)}, bf16[128,128]{0,1:T(8,128)(2,1)S(1)}, u32[]{:S(2)}, u32[]{:S(2)}) collective-permute-start(bf16[128,128]{0,1:T(8,128)(2,1)S(1)} %get-tuple-element.24), channel_id=1, source_target_pairs={{0,8},{8,16},{16,24},{24,32},{32,40},{40,48},{48,56},{56,64},{64,7... | collective-permute-start | bytes 98312 | tf_op jit(solution)/shard_map/ppermute | solution.py:27
  335.1 5.8 %collective-permute-start.19 = (bf16[128,128]{0,1:T(8,128)(2,1)S(1)}, bf16[128,128]{0,1:T(8,128)(2,1)S(1)}, u32[]{:S(2)}, u32[]{:S(2)}) collective-permute-start(bf16[128,128]{0,1:T(8,128)(2,1)S(1)} %get-tuple-element.25), channel_id=1, source_target_pairs={{8,0},{16,8},{24,16},{32,24},{40,32},{48,40},{56,48},{64,56},{72,6... | collective-permute-start | bytes 98312 | tf_op jit(solution)/shard_map/ppermute | solution.py:30
  349.4 44.0 %copy-start.5 = (f32[2048]{0:T(1024)S(1)}, f32[2048]{0:T(1024)}, u32[]{:S(2)}) copy-start(f32[2048]{0:T(1024)} %param.15) | copy-start | bytes 24580
Sparse Core Ops, SparseCore 0:
  10.3 56.4 all-gather.1
  97.1 55.0 reduce-scatter.3
  230.5 53.0 reduce-scatter.5
  353.8 38.3 reduce-scatter.7
